TPU v7x, 32 devices: a whole 2x2x4 slice. The times are simulated.
32 devices in a mesh: sp: 8 (over z, y), tp: 4 (over x, core).
Axes of the slice: x: 2, y: 2, z: 4, core: 2. Of those that a mesh axis runs over, the one named last changes fastest.
Arguments:
- tokens: bfloat16 [4096, 2048], P('sp', 'tp'), may hold values from -6 to 6
- in_gain: float32 [2048], replicated, may hold values from 0.1 to 1.9
- conv_value_w: bfloat16 [2048, 1024], P(None, 'tp'), may hold values from -0.125 to 0.125
- conv_gate_w: bfloat16 [2048, 1024], P(None, 'tp'), may hold values from -0.125 to 0.125
- conv_taps: float32 [31, 1024], P(None, 'tp'), may hold values from -8 to 8
- conv_gain: float32 [1024], P('tp'), may hold values from 0.1 to 1.9
- query_latent_weight: bfloat16 [2048, 512], replicated, may hold values from -0.125 to 0.125
- latent_weight: bfloat16 [2048, 512], replicated, may hold values from -0.125 to 0.125
- rope_key_w: bfloat16 [2048, 64], replicated, may hold values from -0.125 to 0.125
- query_gain: float32 [512], replicated, may hold values from 1.5 to 8, as said below
- latent_gain: float32 [512], replicated, may hold values from 1.5 to 8, as said below
- query_weight: bfloat16 [512, 1024], P(None, 'tp'), may hold values from -0.25 to 0.25
- query_rotary_weight: bfloat16 [512, 512], P(None, 'tp'), may hold values from -0.25 to 0.25
- key_weight: bfloat16 [512, 1024], P(None, 'tp'), may hold values from -0.25 to 0.25
- value_weight: bfloat16 [512, 1024], P(None, 'tp'), may hold values from -0.25 to 0.25
- conv_out_w: bfloat16 [1024, 2048], P('tp'), may hold values from -0.125 to 0.125
- attn_out_w: bfloat16 [1024, 2048], P('tp'), may hold values from -0.125 to 0.125
- out_gain: float32 [2048], replicated, may hold values from 0.1 to 1.9
Outputs:
- mixed: bfloat16 [4096, 2048], P(('sp', 'tp'))
Inputs may be any that keep to these rules, and one draw needn't show every extreme that they name: `query_gain`: positive gains. `latent_gain`: positive gains.
All inputs are finite; a program needn't handle non-finite values.
Results may differ from a plain program's by a relative error of at most 0.018.
The roundings to bfloat16 on the way count: a program that leaves them out, or rounds other values in their place, can miss the bound.
Values may be sent and summed in bfloat16 or wider, within the bound.
A program may use at most 128 MiB of HBM per device.

v0:
```python
import math
import jax
import jax.numpy as jnp
from jax import lax
from jax.sharding import PartitionSpec as P

CONV_CH = 1024
HEAD_WIDTH = 128
norm_eps = 1e-06
layer_eps = 1e-05
rope_base = 10000.0
block_limit = 512


def extended(value, sides, width):
    for axis, dim in sides:
        size, length = (lax.axis_size(axis), value.shape[dim])
        up = [(i, (i + 1) % size) for i in range(size - 1)]
        down = [(j, i) for i, j in up]
        last = lax.slice_in_dim(value, length - width, length, axis=dim)
        leading = lax.slice_in_dim(value, 0, width, axis=dim)
        before = lax.ppermute(last, axis, up)
        after = lax.ppermute(leading, axis, down)
        value = jnp.concatenate([before, value, after], axis=dim)
    return value


def rms_scaled(values, gain):
    return values * lax.rsqrt(jnp.mean(values * values, axis=-1, keepdims=True) + norm_eps) * gain


def rotate(values, cosine_table, sine_table):
    halfway = values.shape[-1] // 2
    first = values[..., :halfway]
    second = values[..., halfway:]
    return jnp.concatenate(
        [first * cosine_table - second * sine_table, second * cosine_table + first * sine_table],
        axis=-1,
    )


def tables(positions, width):
    halfway = width // 2
    inverse = rope_base ** (-jnp.arange(halfway, dtype=jnp.float32) / halfway)
    angles = positions[:, None] * inverse[None, :]
    return (jnp.cos(angles), jnp.sin(angles))


def local(
    tokens,
    in_gain,
    conv_value_w,
    conv_gate_w,
    conv_taps,
    conv_gain,
    query_latent_weight,
    latent_weight,
    rope_key_w,
    query_gain,
    latent_gain,
    query_weight,
    query_rotary_weight,
    key_weight,
    value_weight,
    conv_out_w,
    attn_out_w,
    out_gain,
):
    full_rows = lax.all_gather(tokens, "tp", axis=1, tiled=True)
    tok_here = full_rows.shape[0]
    normed = rms_scaled(full_rows.astype(jnp.float32), in_gain).astype(jnp.bfloat16)
    conv_value = jnp.dot(normed, conv_value_w, preferred_element_type=jnp.float32)
    conv_gate = jnp.dot(normed, conv_gate_w, preferred_element_type=jnp.float32)
    gated = (conv_value * jax.nn.sigmoid(conv_gate)).astype(jnp.bfloat16)
    reach = conv_taps.shape[0] // 2
    padded = extended(gated, (("sp", 0),), reach).astype(jnp.float32)
    convolved = jnp.zeros(gated.shape, jnp.float32)
    for offset_tap in range(conv_taps.shape[0]):
        convolved = convolved + conv_taps[offset_tap] * padded[offset_tap : offset_tap + tok_here]
    stat_sums = lax.psum((jnp.sum(convolved, axis=1), jnp.sum(convolved * convolved, axis=1)), "tp")
    chan_mean = stat_sums[0] / CONV_CH
    chan_square = stat_sums[1] / CONV_CH
    shaped = (
        (convolved - chan_mean[:, None])
        * lax.rsqrt(chan_square - chan_mean * chan_mean + layer_eps)[:, None]
        * conv_gain
    )
    conv_result = jax.nn.silu(shaped).astype(jnp.bfloat16)
    rope_width = rope_key_w.shape[1]
    heads_here = key_weight.shape[1] // HEAD_WIDTH
    score_scale = (HEAD_WIDTH + rope_width) ** (-0.5)
    positions = (lax.axis_index("sp") * tok_here + jnp.arange(tok_here, dtype=jnp.int32)).astype(
        jnp.float32
    )
    cosine_table, sine_table = tables(positions, rope_width)
    query_lat = rms_scaled(
        jnp.dot(normed, query_latent_weight, preferred_element_type=jnp.float32), query_gain
    ).astype(jnp.bfloat16)
    latent = rms_scaled(
        jnp.dot(normed, latent_weight, preferred_element_type=jnp.float32), latent_gain
    ).astype(jnp.bfloat16)
    rope_keys = rotate(
        jnp.dot(normed, rope_key_w, preferred_element_type=jnp.float32), cosine_table, sine_table
    ).astype(jnp.bfloat16)
    query_main = (
        jnp.dot(query_lat, query_weight, preferred_element_type=jnp.float32)
        .astype(jnp.bfloat16)
        .reshape(tok_here, heads_here, HEAD_WIDTH)
    )
    query_rope = rotate(
        jnp.dot(query_lat, query_rotary_weight, preferred_element_type=jnp.float32).reshape(
            tok_here, heads_here, rope_width
        ),
        cosine_table[:, None, :],
        sine_table[:, None, :],
    ).astype(jnp.bfloat16)

    def attend(state, key_rows, rope_rows, value_rows):
        running_max, running_sum, accum = state
        scores = (
            jnp.einsum("thd,phd->htp", query_main, key_rows, preferred_element_type=jnp.float32)
            + jnp.einsum("thr,pr->htp", query_rope, rope_rows, preferred_element_type=jnp.float32)
        ) * score_scale
        new_max = jnp.maximum(running_max, jnp.max(scores, axis=-1))
        rescale = jnp.exp(running_max - new_max)
        weights = jnp.exp(scores - new_max[:, :, None])
        running_sum = running_sum * rescale + jnp.sum(weights, axis=-1)
        accum = accum * rescale.T[:, :, None] + jnp.einsum(
            "htp,phd->thd",
            weights.astype(jnp.bfloat16),
            value_rows,
            preferred_element_type=jnp.float32,
        )
        return (new_max, running_sum, accum)

    start_state = (
        jnp.full((heads_here, tok_here), -1e30, jnp.float32),
        jnp.zeros((heads_here, tok_here), jnp.float32),
        jnp.zeros((tok_here, heads_here, HEAD_WIDTH), jnp.float32),
    )
    state = start_state
    arrays = (
        lax.all_gather(latent, "sp", axis=0, tiled=True),
        lax.all_gather(rope_keys, "sp", axis=0, tiled=True),
    )
    count = arrays[0].shape[0]
    block_rows = math.gcd(count, block_limit)
    stacked = tuple(
        (member.reshape((count // block_rows, block_rows) + member.shape[1:]) for member in arrays)
    )

    def block_step(inner, pieces):
        latent_rows, rope_rows = pieces
        key_rows = jnp.dot(latent_rows, key_weight, preferred_element_type=jnp.float32).astype(
            jnp.bfloat16
        )
        value_flat = jnp.dot(latent_rows, value_weight, preferred_element_type=jnp.float32).astype(
            jnp.bfloat16
        )
        key_rows = key_rows.reshape(block_rows, heads_here, HEAD_WIDTH)
        value_rows = value_flat.reshape(block_rows, heads_here, HEAD_WIDTH)
        return (attend(inner, key_rows, rope_rows, value_rows), None)

    state, unused = lax.scan(block_step, state, stacked)
    running_max, running_sum, accum = state
    attention_result = (
        (accum / running_sum.T[:, :, None])
        .astype(jnp.bfloat16)
        .reshape(tok_here, heads_here * HEAD_WIDTH)
    )
    summed = jnp.dot(conv_result, conv_out_w, preferred_element_type=jnp.float32) + jnp.dot(
        attention_result, attn_out_w, preferred_element_type=jnp.float32
    )
    merged = lax.psum_scatter(
        lax.optimization_barrier(summed.astype(jnp.bfloat16))
        .astype(jnp.float32)
        .astype(jnp.bfloat16),
        "tp",
        scatter_dimension=0,
        tiled=True,
    ).astype(jnp.float32)
    return rms_scaled(merged, out_gain).astype(jnp.bfloat16)


def solution(mesh):
    return jax.shard_map(
        local,
        mesh=mesh,
        in_specs=(
            P("sp", "tp"),
            P(),
            P(None, "tp"),
            P(None, "tp"),
            P(None, "tp"),
            P("tp"),
            P(),
            P(),
            P(),
            P(),
            P(),
            P(None, "tp"),
            P(None, "tp"),
            P(None, "tp"),
            P(None, "tp"),
            P("tp", None),
            P("tp", None),
            P(),
        ),
        out_specs=P(("sp", "tp"), None),
        check_vma=False,
    )
```

profile of v0, /device:TPU:0, one launch (start us, length us, event | category | flops | bytes accessed | tf_op | source)
XLA Modules:
  0.0 212.8 jit_solution(5674878979856486515)
XLA Ops:
  7.3 26.9 %all-gather.3.cloned.1.call-done = bf16[512,2048]{1,0:T(8,128)(2,1)} async-done(((bf16[512,512]{1,0:T(8,128)(2,1)}), bf16[512,2048]{1,0:T(8,128)(2,1)}) %all-gather.3.cloned.1.call-update) | async-done | bytes 2097168 | tf_op jit(solution)/shard_map/all_gather | solution.py:69
  34.2 2.2 %fusion.18 = f32[512]{0:T(512)S(1)} fusion(bf16[512,2048]{1,0:T(8,128)(2,1)} %all-gather.3.cloned.1.call-done), kind=kLoop, calls=%fused_computation.28 | loop fusion | flops 3145216 | bytes 2099200 | tf_op jit(solution)/shard_map/reduce_sum | solution.py:29
  36.5 1.4 multiply_reduce_fusion.1
  40.4 2.8 %fusion.23 = f32[512,256]{1,0:T(8,128)S(1)} fusion(bf16[2048,256]{1,0:T(8,128)(2,1)} %param.23, bf16[512,2048]{1,0:T(8,128)(2,1)} %all-gather.3.cloned.1.call-done, f32[2048]{0:T(1024)S(1)} %copy-done.14, f32[512]{0:T(512)S(1)} %add_rsqrt_fusion.3), kind=kOutput, calls=%fused_computation.38 | convolution fusion | flops 541458432 | bytes 3680256 | tf_op jit(solution)/shard_map/dot_general | solution.py:73
  44.6 3.4 %collective-permute-start = (bf16[15,256]{1,0:T(8,128)(2,1)}, bf16[15,256]{1,0:T(8,128)(2,1)S(1)}, u32[]{:S(2)}, u32[]{:S(2)}) collective-permute-start(bf16[15,256]{1,0:T(8,128)(2,1)} %get-tuple-element.134), channel_id=1, source_target_pairs={{0,4},{4,8},{8,12},{12,16},{16,20},{20,24},{24,28},{1,5},{5,9},{9,... | collective-permute-start | bytes 23048 | tf_op jit(solution)/shard_map/ppermute | solution.py:22
  48.0 1.4 collective-permute-start.1
  50.7 1.5 multiply_reduce_fusion
  52.2 35.2 %all_gather.11 = bf16[4096,64]{0,1:T(8,128)(2,1)S(1)} all-gather(bf16[512,64]{0,1:T(8,128)(2,1)S(1)} %pad_maximum_fusion.1), channel_id=1, replica_groups=mesh['sp'=8,'tp'=4] {'sp'}, dimensions={0}, use_global_device_ids=true | all-gather | bytes 589824 | tf_op jit(solution)/shard_map/all_gather | solution.py:144
  90.1 3.3 %fusion.73 = (f32[512]{0:T(512)S(1)}, f32[512]{0:T(512)S(1)}, f32[512,256]{1,0:T(8,128)S(1)}) fusion(f32[542,256]{1,0:T(8,128)S(1)} %maximum_convert_fusion, f32[256]{0:T(256)} %bitcast.126, f32[256]{0:T(256)} %bitcast.127, f32[256]{0:T(256)} %bitcast.129, f32[256]{0:T(256)} %bitcast.130, f32[256]{0:T(256)} %bitcast.131, f32[256]{0:T(256)} %bitcast.132, ...), kind=kLoop, calls=%fused_computation.140 | loop fusion | flops 8387584 | bytes 16813056 | tf_op jit(solution)/shard_map/reduce_sum | solution.py:80
  93.5 6.8 %all-reduce = (f32[512]{0:T(512)}, f32[512]{0:T(512)}) all-reduce(f32[512]{0:T(512)S(1)} %get-tuple-element.104, f32[512]{0:T(512)S(1)} %get-tuple-element.103), channel_id=1, replica_groups=mesh['sp'=8,'tp'=4] {'tp'}, use_global_device_ids=true, to_apply=%region_4.0 | all-reduce | flops 1024 | bytes 8192 | tf_op jit(solution)/shard_map/psum | solution.py:80
  101.0 4.0 %fusion.58 = f32[512,2048]{1,0:T(8,128)} fusion(bf16[256,2048]{1,0:T(8,128)(2,1)} %param.35, f32[512,256]{1,0:T(8,128)S(1)} %get-tuple-element.129, f32[256]{0:T(256)} %param.25, f32[512]{0:T(512)S(1)} %get-tuple-element.174, f32[512]{0:T(512)S(1)} %get-tuple-element.173), kind=kOutput, calls=%fused_computation.114 | convolution fusion | flops 537919488 | bytes 5772288 | tf_op jit(solution)/shard_map/dot_general | solution.py:171
  105.0 12.6 %all-gather.5.cloned.1.call-done = bf16[4096,512]{0,1:T(8,128)(2,1)} async-done(((bf16[512,512]{0,1:T(8,128)(2,1)}), bf16[4096,512]{0,1:T(8,128)(2,1)}) %all-gather.5.cloned.1.call-update) | async-done | bytes 4194320 | tf_op jit(solution)/shard_map/all_gather | solution.py:143
  117.6 6.4 %copy.26 = bf16[4096,512]{1,0:T(8,128)(2,1)} copy(bf16[4096,512]{0,1:T(8,128)(2,1)} %all-gather.5.cloned.1.call-done) | data formatting | bytes 8388608
  124.1 44.4 %while.15 = (s32[]{:T(128)}, f32[2,512]{1,0:T(2,128)S(1)}, f32[2,512]{1,0:T(2,128)S(1)}, f32[512,2,128]{0,2,1:T(8,128)S(1)}, bf16[8,512,512]{2,1,0:T(8,128)(2,1)...) while((s32[]{:T(128)}, f32[2,512]{1,0:T(2,128)S(1)}, ...), condition=%wide.region_10.11_spmd.clone, body=%wide.region_7.10_spmd.clone.sunk | while | flops 608311296 | bytes 14680213 | solution.py:164
  124.1 1.4 convolution_convert_fusion.6
  125.5 1.4 convolution_convert_fusion.5
  129.6 1.4 convolution_convert_fusion.6
  131.0 1.4 convolution_convert_fusion.5
  135.2 1.4 convolution_convert_fusion.6
  136.6 1.4 convolution_convert_fusion.5
  140.7 1.4 convolution_convert_fusion.6
  142.1 1.4 convolution_convert_fusion.5
  146.3 1.4 convolution_convert_fusion.6
  147.7 1.4 convolution_convert_fusion.5
  151.8 1.4 convolution_convert_fusion.6
  153.2 1.4 convolution_convert_fusion.5
  157.4 1.4 convolution_convert_fusion.6
  158.8 1.4 convolution_convert_fusion.5
  164.3 1.4 convolution_convert_fusion.5
  168.5 4.6 %add_convert_fusion = bf16[512,2048]{1,0:T(8,128)(2,1)} fusion(f32[512,2048]{1,0:T(8,128)} %fusion.58, bf16[512,256]{0,1:T(8,128)(2,1)S(1)} %bitcast.114, bf16[256,2048]{1,0:T(8,128)(2,1)} %param.36), kind=kOutput, calls=%fused_computation.31 | convolution fusion | flops 538968064 | bytes 7602176 | tf_op jit(solution)/shard_map/dot_general | solution.py:171
  173.1 29.9 %reduce-scatter.2.cloned.1.call-done = bf16[128,2048]{1,0:T(8,128)(2,1)} async-done(((bf16[512,2048]{1,0:T(8,128)(2,1)}), bf16[128,2048]{1,0:T(8,128)(2,1)}) %reduce-scatter.2.cloned.1.call-update) | async-done | bytes 524304 | tf_op jit(solution)/shard_map/reduce_scatter | solution.py:174
  204.3 2.0 fusion.27
  (124 shorter events, 33.4 us)
Async XLA Ops:
  6.5 29.9 %copy-start = (bf16[2048,512]{1,0:T(8,128)(2,1)S(1)}, bf16[2048,512]{1,0:T(8,128)(2,1)}, u32[]{:S(2)}) copy-start(bf16[2048,512]{1,0:T(8,128)(2,1)} %param.27) | copy-start | bytes 6291460
  6.5 29.9 %copy-start.14 = (f32[2048]{0:T(1024)S(1)}, f32[2048]{0:T(1024)}, u32[]{:S(2)}) copy-start(f32[2048]{0:T(1024)} %param.21) | copy-start | bytes 24580
  6.5 27.7 %all-gather.3.cloned.1.call-start = ((), (), s32[]{:S(2)}) async-start(), calls=%async_computation.1 | async-start | bytes 2621440 | tf_op jit(solution)/shard_map/all_gather | solution.py:69
  7.3 110.4 %all-gather.5.cloned.1.call-start = ((), (), s32[]{:S(2)}) async-start(), calls=%async_computation.2 | async-start | bytes 4718592 | tf_op jit(solution)/shard_map/all_gather | solution.py:143
  34.2 2.3 %copy-start.3 = (bf16[512,2048]{1,0:T(8,128)(2,1)S(1)}, bf16[512,2048]{1,0:T(8,128)(2,1)}, u32[]{:S(2)}) copy-start(bf16[512,2048]{1,0:T(8,128)(2,1)} %all-gather.3.cloned.1.call-done) | copy-start | bytes 6291460
  36.5 1.5 copy-start.10
  37.9 1.1 copy-start.7
  38.9 164.1 %reduce-scatter.2.cloned.1.call-start = ((), (), s32[]{:S(2)}) async-start(), calls=%async_computation.3 | async-start | bytes 2621440 | tf_op jit(solution)/shard_map/reduce_scatter | solution.py:174
  40.4 2.8 %copy-start.4 = (bf16[512,2048]{1,0:T(8,128)(2,1)S(1)}, bf16[512,2048]{1,0:T(8,128)(2,1)}, u32[]{:S(2)}) copy-start(bf16[512,2048]{1,0:T(8,128)(2,1)} %all-gather.3.cloned.1.call-done) | copy-start | bytes 6291460
  40.4 2.8 %copy-start.12 = (bf16[2048,256]{1,0:T(8,128)(2,1)S(1)}, bf16[2048,256]{1,0:T(8,128)(2,1)}, u32[]{:S(2)}) copy-start(bf16[2048,256]{1,0:T(8,128)(2,1)} %param.22) | copy-start | bytes 3145732
  43.2 6.3 %copy-start.13 = (bf16[2048,64]{0,1:T(8,128)(2,1)S(1)}, bf16[2048,64]{0,1:T(8,128)(2,1)}, u32[]{:S(2)}) copy-start(bf16[2048,64]{0,1:T(8,128)(2,1)} %param.28) | copy-start | bytes 786436
  44.6 44.7 %collective-permute-start = (bf16[15,256]{1,0:T(8,128)(2,1)}, bf16[15,256]{1,0:T(8,128)(2,1)S(1)}, u32[]{:S(2)}, u32[]{:S(2)}) collective-permute-start(bf16[15,256]{1,0:T(8,128)(2,1)} %get-tuple-element.134), channel_id=1, source_target_pairs={{0,4},{4,8},{8,12},{12,16},{16,20},{20,24},{24,28},{1,5},{5,9},{9,... | collective-permute-start | bytes 23048 | tf_op jit(solution)/shard_map/ppermute | solution.py:22
  48.0 2.7 %copy-start.11 = (bf16[2048,512]{1,0:T(8,128)(2,1)S(1)}, bf16[2048,512]{1,0:T(8,128)(2,1)}, u32[]{:S(2)}) copy-start(bf16[2048,512]{1,0:T(8,128)(2,1)} %param.26) | copy-start | bytes 6291460
  48.0 2.7 %copy-start.15 = (f32[2048]{0:T(1024)S(1)}, f32[2048]{0:T(1024)}, u32[]{:S(2)}) copy-start(f32[2048]{0:T(1024)} %param.21) | copy-start | bytes 24580
  48.0 41.3 %collective-permute-start.1 = (bf16[15,256]{1,0:T(8,128)(2,1)}, bf16[15,256]{1,0:T(8,128)(2,1)}, u32[]{:S(2)}, u32[]{:S(2)}) collective-permute-start(bf16[15,256]{1,0:T(8,128)(2,1)} %get-tuple-element.135), channel_id=1, source_target_pairs={{4,0},{8,4},{12,8},{16,12},{20,16},{24,20},{28,24},{5,1},{9,5},{13... | collective-permute-start | bytes 23048 | tf_op jit(solution)/shard_map/ppermute | solution.py:23
  50.7 36.8 %copy-start.6 = (bf16[512,128]{1,0:T(8,128)(2,1)S(1)}, bf16[512,128]{1,0:T(8,128)(2,1)}, u32[]{:S(2)}) copy-start(bf16[512,128]{1,0:T(8,128)(2,1)} %param.32) | copy-start | bytes 393220
  50.7 36.7 %copy-start.9 = (f32[512]{0:T(512)S(1)}, f32[512]{0:T(512)}, u32[]{:S(2)}) copy-start(f32[512]{0:T(512)} %param.29) | copy-start | bytes 6148
  52.2 35.7 %copy-start.5 = (bf16[512,256]{1,0:T(8,128)(2,1)S(1)}, bf16[512,256]{1,0:T(8,128)(2,1)}, u32[]{:S(2)}) copy-start(bf16[512,256]{1,0:T(8,128)(2,1)} %param.31) | copy-start | bytes 786436
  105.0 19.1 %copy-start.1 = (bf16[512,256]{1,0:T(8,128)(2,1)S(1)}, bf16[512,256]{1,0:T(8,128)(2,1)}, u32[]{:S(2)}) copy-start(bf16[512,256]{1,0:T(8,128)(2,1)} %param.33) | copy-start | bytes 786436
  105.0 19.1 %copy-start.2 = (bf16[512,256]{1,0:T(8,128)(2,1)S(1)}, bf16[512,256]{1,0:T(8,128)(2,1)}, u32[]{:S(2)}) copy-start(bf16[512,256]{1,0:T(8,128)(2,1)} %param.34) | copy-start | bytes 786436
  173.1 31.1 %copy-start.8 = (f32[2048]{0:T(1024)S(1)}, f32[2048]{0:T(1024)}, u32[]{:S(2)}) copy-start(f32[2048]{0:T(1024)} %param.37) | copy-start | bytes 24580
Sparse Core Ops, SparseCore 0:
  8.9 25.2 all-gather.2
  39.1 78.5 all-gather.4
  173.3 29.7 reduce-scatter.1
where the time goes:
time: 214 us; the launch traced here: 213 us
  waiting for transfers between devices  70.2 us (33%)
  matrix products  57.8 us (27%)
  blocking collectives  42.1 us (20%)
  other arithmetic  14.4 us (7%)
  between operations  13.5 us (6%)
  local copies, waits for them, and re-layouts  9.48 us (4%)
  starting transfers between devices  4.89 us (2%)
    all_gather x1, blocking collectives, local(): lax.all_gather(rope_keys, 'sp', axis=0, tiled=True)  35.2 us
    reduce_scatter x1, waiting for transfers between devices, local(): lax.psum_scatter(lax.optimization_barrier(summed.astype(jnp.bfloat16)).as...  29.9 us
    all_gather x1, waiting for transfers between devices, local(): full_rows = lax.all_gather(tokens, 'tp', axis=1, tiled=True)  26.9 us
    all_gather x1, waiting for transfers between devices, local(): lax.all_gather(latent, 'sp', axis=0, tiled=True)  12.6 us
    dot_general x8, matrix products, block_step(): jnp.dot(latent_rows, key_weight, preferred_element_type=jnp.float32)  11.1 us
    dot_general x8, matrix products, block_step(): jnp.dot(latent_rows, value_weight, preferred_element_type=jnp.float32)  11.1 us
    dot_general x8, matrix products, attend(): jnp.einsum('thr,pr->htp', query_rope, rope_rows, preferred_element_type=j...  10.5 us
    psum x1, blocking collectives, local(): lax.psum((jnp.sum(convolved, axis=1), jnp.sum(convolved * convolved, axis...  6.83 us
  transfers between devices with their start and end apart: 5, of which 3 were waited for; matrix products, arithmetic and copies ran while one was open for 9% of the time, Pallas kernels for 0%

commit v1 on v0

--- a/solution.py
+++ b/solution.py
@@ -66,7 +66,12 @@
     attn_out_w,
     out_gain,
 ):
-    full_rows = lax.all_gather(tokens, "tp", axis=1, tiled=True)
+    ring = [tokens]
+    for hop in range(3):
+        ring.append(lax.ppermute(ring[-1], "tp", [(dev, (dev + 1) % 4) for dev in range(4)]))
+    full_rows = jnp.roll(
+        jnp.concatenate(ring[::-1], axis=1), (lax.axis_index("tp") + 1) * ring[0].shape[1], axis=1
+    )
     tok_here = full_rows.shape[0]
     normed = rms_scaled(full_rows.astype(jnp.float32), in_gain).astype(jnp.bfloat16)
     conv_value = jnp.dot(normed, conv_value_w, preferred_element_type=jnp.float32)

time: 214 us -> 221 us (1.033)
  local copies, waits for them, and re-layouts: 9.48 us -> 15.8 us
    all_gather x1 -> x0, waiting for transfers between devices: 26.9 us -> none  [local(): full_rows = lax.all_gather(tokens, 'tp', axis=1, tiled=True)]
    ppermute x0 -> x3, waiting for transfers between devices: none -> 26.6 us  [local(): lax.ppermute(ring[-1], 'tp', [(dev, (dev + 1) % 4) for dev in range(4)])]
    unnamed x34 -> x45, local copies, waits for them, and re-layouts: 6.7 us -> 12.9 us
  transfers between devices with their start and end apart: 5 -> 7, of which waited for: 3 -> 5; matrix products, arithmetic and copies ran while one was open for 9% -> 9% of each run, Pallas kernels for 0% -> 0%
where the time goes in v1:
time: 221 us; the launch traced here: 219 us
  waiting for transfers between devices  69.1 us (31%)
  matrix products  58.6 us (27%)
  blocking collectives  42.4 us (19%)
  local copies, waits for them, and re-layouts  15.8 us (7%)
  between operations  13.8 us (6%)
  other arithmetic  12.7 us (6%)
  starting transfers between devices  6.17 us (3%)
    all_gather x1, blocking collectives, local(): lax.all_gather(rope_keys, 'sp', axis=0, tiled=True)  35.6 us
    reduce_scatter x1, waiting for transfers between devices, local(): lax.psum_scatter(lax.optimization_barrier(summed.astype(jnp.bfloat16)).as...  30.2 us
    ppermute x3, waiting for transfers between devices, local(): lax.ppermute(ring[-1], 'tp', [(dev, (dev + 1) % 4) for dev in range(4)])  26.6 us
    unnamed x45, local copies, waits for them, and re-layouts  12.9 us
    all_gather x1, waiting for transfers between devices, local(): lax.all_gather(latent, 'sp', axis=0, tiled=True)  12.2 us
    dot_general x8, matrix products, block_step(): jnp.dot(latent_rows, key_weight, preferred_element_type=jnp.float32)  11.1 us
    dot_general x8, matrix products, block_step(): jnp.dot(latent_rows, value_weight, preferred_element_type=jnp.float32)  11.1 us
    dot_general x8, matrix products, attend(): jnp.einsum('thr,pr->htp', query_rope, rope_rows, preferred_element_type=j...  10.5 us
  transfers between devices with their start and end apart: 7, of which 5 were waited for; matrix products, arithmetic and copies ran while one was open for 9% of the time, Pallas kernels for 0%

profile of v1, /device:TPU:0, one launch (start us, length us, event | category | flops | bytes accessed | tf_op | source)
XLA Modules:
  0.0 219.1 jit_solution(15810371532290973835)
XLA Ops:
  7.0 9.0 %collective-permute-done = bf16[512,512]{1,0:T(8,128)(2,1)S(1)} collective-permute-done((bf16[512,512]{1,0:T(8,128)(2,1)}, bf16[512,512]{1,0:T(8,128)(2,1)S(1)}, u32[]{:S(2)}, u32[]{:S(2)}) %collective-permute-start) | collective-permute-done | bytes 524320 | tf_op jit(solution)/shard_map/ppermute | solution.py:71
  16.1 8.7 %collective-permute-done.1 = bf16[512,512]{1,0:T(8,128)(2,1)} collective-permute-done((bf16[512,512]{1,0:T(8,128)(2,1)S(1)}, bf16[512,512]{1,0:T(8,128)(2,1)}, u32[]{:S(2)}, u32[]{:S(2)}) %collective-permute-start.1) | collective-permute-done | bytes 524320 | tf_op jit(solution)/shard_map/ppermute | solution.py:71
  24.8 8.9 %collective-permute-done.2 = bf16[512,512]{1,0:T(8,128)(2,1)} collective-permute-done((bf16[512,512]{1,0:T(8,128)(2,1)}, bf16[512,512]{1,0:T(8,128)(2,1)}, u32[]{:S(2)}, u32[]{:S(2)}) %collective-permute-start.2) | collective-permute-done | bytes 524320 | tf_op jit(solution)/shard_map/ppermute | solution.py:71
  40.0 1.5 multiply_reduce_fusion.1
  43.9 2.8 %fusion.23 = f32[512,256]{1,0:T(8,128)S(1)} fusion(bf16[2048,256]{1,0:T(8,128)(2,1)} %param.23, f32[2048]{0:T(1024)S(1)} %copy-done.16, f32[512]{0:T(512)S(1)} %add_rsqrt_fusion.3, bf16[512,4096]{1,0:T(8,128)(2,1)} %copy-done.4, s32[]{:T(128)S(6)} %select_n.14), kind=kOutput, calls=%fused_computation.38 | convolution fusion | flops 541458432 | bytes 3680260 | tf_op jit(solution)/shard_map/dot_general | solution.py:78
  48.7 4.3 %collective-permute-start.3 = (bf16[15,256]{1,0:T(8,128)(2,1)}, bf16[15,256]{1,0:T(8,128)(2,1)S(1)}, u32[]{:S(2)}, u32[]{:S(2)}) collective-permute-start(bf16[15,256]{1,0:T(8,128)(2,1)} %get-tuple-element.134), channel_id=1, source_target_pairs={{0,4},{4,8},{8,12},{12,16},{16,20},{20,24},{24,28},{1,5},{5,9},{9,... | collective-permute-start | bytes 23048 | tf_op jit(solution)/shard_map/ppermute | solution.py:22
  55.6 2.2 %multiply_reduce_fusion = (f32[512]{0:T(512)S(1)}, f32[512,512]{0,1:T(8,128)S(1)}) fusion(bf16[2048,512]{1,0:T(8,128)(2,1)S(1)} %copy-done.13, f32[2048]{0:T(1024)S(1)} %copy-done.17, f32[512]{0:T(512)} %copy-done.12, bf16[512,4096]{1,0:T(8,128)(2,1)S(1)} %copy-done.5, s32[]{:T(128)S(6)} %select_n.14), kind=kOutput, calls=%fused_computation.45 | convolution fusion | flops 1078459904 | bytes 5255172 | tf_op jit(solution)/shard_map/dot_general | solution.py:102
  57.9 35.6 %all_gather.7 = bf16[4096,64]{0,1:T(8,128)(2,1)S(1)} all-gather(bf16[512,64]{0,1:T(8,128)(2,1)S(1)} %pad_maximum_fusion.1), channel_id=1, replica_groups=mesh['sp'=8,'tp'=4] {'sp'}, dimensions={0}, use_global_device_ids=true | all-gather | bytes 589824 | tf_op jit(solution)/shard_map/all_gather | solution.py:149
  96.1 3.3 %fusion.73 = (f32[512]{0:T(512)S(1)}, f32[512]{0:T(512)S(1)}, f32[512,256]{1,0:T(8,128)S(1)}) fusion(f32[542,256]{1,0:T(8,128)S(1)} %maximum_convert_fusion, f32[256]{0:T(256)} %bitcast.126, f32[256]{0:T(256)} %bitcast.127, f32[256]{0:T(256)} %bitcast.129, f32[256]{0:T(256)} %bitcast.130, f32[256]{0:T(256)} %bitcast.131, f32[256]{0:T(256)} %bitcast.132, ...), kind=kLoop, calls=%fused_computation.148 | loop fusion | flops 8387584 | bytes 16813056 | tf_op jit(solution)/shard_map/reduce_sum | solution.py:85
  99.5 6.8 %all-reduce = (f32[512]{0:T(512)}, f32[512]{0:T(512)}) all-reduce(f32[512]{0:T(512)S(1)} %get-tuple-element.104, f32[512]{0:T(512)S(1)} %get-tuple-element.103), channel_id=1, replica_groups=mesh['sp'=8,'tp'=4] {'tp'}, use_global_device_ids=true, to_apply=%region_4.5 | all-reduce | flops 1024 | bytes 8192 | tf_op jit(solution)/shard_map/psum | solution.py:85
  107.0 4.0 %fusion.58 = f32[512,2048]{1,0:T(8,128)} fusion(bf16[256,2048]{1,0:T(8,128)(2,1)} %param.35, f32[512,256]{1,0:T(8,128)S(1)} %get-tuple-element.129, f32[256]{0:T(256)} %param.25, f32[512]{0:T(512)S(1)} %get-tuple-element.174, f32[512]{0:T(512)S(1)} %get-tuple-element.173), kind=kOutput, calls=%fused_computation.114 | convolution fusion | flops 537919488 | bytes 5772288 | tf_op jit(solution)/shard_map/dot_general | solution.py:176
  111.0 12.2 %all-gather.2.cloned.1.call-done = bf16[4096,512]{0,1:T(8,128)(2,1)} async-done(((bf16[512,512]{0,1:T(8,128)(2,1)}), bf16[4096,512]{0,1:T(8,128)(2,1)}) %all-gather.2.cloned.1.call-update) | async-done | bytes 4194320 | tf_op jit(solution)/shard_map/all_gather | solution.py:148
  123.3 6.5 %copy.26 = bf16[4096,512]{1,0:T(8,128)(2,1)} copy(bf16[4096,512]{0,1:T(8,128)(2,1)} %all-gather.2.cloned.1.call-done) | data formatting | bytes 8388608
  129.7 44.4 %while.15 = (s32[]{:T(128)}, f32[2,512]{1,0:T(2,128)S(1)}, f32[2,512]{1,0:T(2,128)S(1)}, f32[512,2,128]{0,2,1:T(8,128)S(1)}, bf16[8,512,512]{2,1,0:T(8,128)(2,1)...) while((s32[]{:T(128)}, f32[2,512]{1,0:T(2,128)S(1)}, ...), condition=%wide.region_10.11_spmd.clone, body=%wide.region_7.10_spmd.clone.sunk | while | flops 608311296 | bytes 14680213 | solution.py:169
  129.7 1.4 convolution_convert_fusion.6
  131.1 1.4 convolution_convert_fusion.5
  135.3 1.4 convolution_convert_fusion.6
  136.7 1.4 convolution_convert_fusion.5
  140.8 1.4 convolution_convert_fusion.6
  142.2 1.4 convolution_convert_fusion.5
  146.4 1.4 convolution_convert_fusion.6
  147.8 1.4 convolution_convert_fusion.5
  151.9 1.4 convolution_convert_fusion.6
  153.3 1.4 convolution_convert_fusion.5
  157.5 1.4 convolution_convert_fusion.6
  158.9 1.4 convolution_convert_fusion.5
  163.0 1.4 convolution_convert_fusion.6
  164.4 1.4 convolution_convert_fusion.5
  170.0 1.4 convolution_convert_fusion.5
  174.2 4.6 %add_convert_fusion = bf16[512,2048]{1,0:T(8,128)(2,1)} fusion(f32[512,2048]{1,0:T(8,128)} %fusion.58, bf16[512,256]{0,1:T(8,128)(2,1)S(1)} %bitcast.114, bf16[256,2048]{1,0:T(8,128)(2,1)} %param.36), kind=kOutput, calls=%fused_computation.31 | convolution fusion | flops 538968064 | bytes 7602176 | tf_op jit(solution)/shard_map/dot_general | solution.py:176
  178.8 30.2 %reduce-scatter.2.cloned.1.call-done = bf16[128,2048]{1,0:T(8,128)(2,1)} async-done(((bf16[512,2048]{1,0:T(8,128)(2,1)}), bf16[128,2048]{1,0:T(8,128)(2,1)}) %reduce-scatter.2.cloned.1.call-update) | async-done | bytes 524304 | tf_op jit(solution)/shard_map/reduce_scatter | solution.py:179
  210.3 2.0 fusion.27
  (139 shorter events, 41.2 us)
Async XLA Ops:
  6.5 33.4 %copy-start = (bf16[2048,512]{1,0:T(8,128)(2,1)S(1)}, bf16[2048,512]{1,0:T(8,128)(2,1)}, u32[]{:S(2)}) copy-start(bf16[2048,512]{1,0:T(8,128)(2,1)} %param.27) | copy-start | bytes 6291460
  6.5 32.8 %copy-start.3 = (bf16[512,512]{1,0:T(8,128)(2,1)S(1)}, bf16[512,512]{1,0:T(8,128)(2,1)}, u32[]{:S(2)}) copy-start(bf16[512,512]{1,0:T(8,128)(2,1)} %param.20) | copy-start | bytes 1572868
  6.5 116.7 %all-gather.2.cloned.1.call-start = ((), (), s32[]{:S(2)}) async-start(), calls=%async_computation.1 | async-start | bytes 4718592 | tf_op jit(solution)/shard_map/all_gather | solution.py:148
  6.5 9.5 %collective-permute-start = (bf16[512,512]{1,0:T(8,128)(2,1)}, bf16[512,512]{1,0:T(8,128)(2,1)S(1)}, u32[]{:S(2)}, u32[]{:S(2)}) collective-permute-start(bf16[512,512]{1,0:T(8,128)(2,1)} %param.20), channel_id=1, source_target_pairs={{0,1},{1,2},{2,3},{3,0},{4,5},{5,6},{6,7},{7,4},{8,9},{9,10},{10,1... | collective-permute-start | bytes 1572872 | tf_op jit(solution)/shard_map/ppermute | solution.py:71
  16.1 8.7 %collective-permute-start.1 = (bf16[512,512]{1,0:T(8,128)(2,1)S(1)}, bf16[512,512]{1,0:T(8,128)(2,1)}, u32[]{:S(2)}, u32[]{:S(2)}) collective-permute-start(bf16[512,512]{1,0:T(8,128)(2,1)S(1)} %collective-permute-done), channel_id=1, source_target_pairs={{0,1},{1,2},{2,3},{3,0},{4,5},{5,6},{6,7},{7,4},{8,9},{9,10},{10,1... | collective-permute-start | bytes 1572872 | tf_op jit(solution)/shard_map/ppermute | solution.py:71
  24.8 8.9 %collective-permute-start.2 = (bf16[512,512]{1,0:T(8,128)(2,1)}, bf16[512,512]{1,0:T(8,128)(2,1)}, u32[]{:S(2)}, u32[]{:S(2)}) collective-permute-start(bf16[512,512]{1,0:T(8,128)(2,1)} %collective-permute-done.1), channel_id=1, source_target_pairs={{0,1},{1,2},{2,3},{3,0},{4,5},{5,6},{6,7},{7,4},{8,9},{9,10},{10,1... | collective-permute-start | bytes 1572872 | tf_op jit(solution)/shard_map/ppermute | solution.py:71
  35.9 4.0 %copy-start.16 = (f32[2048]{0:T(1024)S(1)}, f32[2048]{0:T(1024)}, u32[]{:S(2)}) copy-start(f32[2048]{0:T(1024)} %param.21) | copy-start | bytes 24580
  39.4 2.0 copy-start.4
  40.0 14.4 %copy-start.12 = (f32[512]{0:T(512)}, f32[512]{0:T(512)S(1)}, u32[]{:S(2)}) copy-start(f32[512]{0:T(512)S(1)} %add_rsqrt_fusion.3) | copy-start | bytes 6148
  40.0 1.5 copy-start.11
  40.0 2.6 %copy-start.8 = (f32[31,256]{1,0:T(8,128)S(1)}, f32[31,256]{1,0:T(8,128)}, u32[]{:S(2)}) copy-start(f32[31,256]{1,0:T(8,128)} %param.24) | copy-start | bytes 95236
  42.5 166.6 %reduce-scatter.2.cloned.1.call-start = ((), (), s32[]{:S(2)}) async-start(), calls=%async_computation.2 | async-start | bytes 2621440 | tf_op jit(solution)/shard_map/reduce_scatter | solution.py:179
  43.9 3.1 %copy-start.5 = (bf16[512,4096]{1,0:T(8,128)(2,1)S(1)}, bf16[512,4096]{1,0:T(8,128)(2,1)}, u32[]{:S(2)}) copy-start(bf16[512,4096]{1,0:T(8,128)(2,1)} %copy-done.4) | copy-start | bytes 12582916
  43.9 3.4 %copy-start.14 = (bf16[2048,256]{1,0:T(8,128)(2,1)S(1)}, bf16[2048,256]{1,0:T(8,128)(2,1)}, u32[]{:S(2)}) copy-start(bf16[2048,256]{1,0:T(8,128)(2,1)} %param.22) | copy-start | bytes 3145732
  47.3 7.1 %copy-start.15 = (bf16[2048,64]{0,1:T(8,128)(2,1)S(1)}, bf16[2048,64]{0,1:T(8,128)(2,1)}, u32[]{:S(2)}) copy-start(bf16[2048,64]{0,1:T(8,128)(2,1)} %param.28) | copy-start | bytes 786436
  48.1 7.5 %copy-start.13 = (bf16[2048,512]{1,0:T(8,128)(2,1)S(1)}, bf16[2048,512]{1,0:T(8,128)(2,1)}, u32[]{:S(2)}) copy-start(bf16[2048,512]{1,0:T(8,128)(2,1)} %param.26) | copy-start | bytes 6291460
  48.1 7.5 %copy-start.17 = (f32[2048]{0:T(1024)S(1)}, f32[2048]{0:T(1024)}, u32[]{:S(2)}) copy-start(f32[2048]{0:T(1024)} %param.21) | copy-start | bytes 24580
  48.7 46.6 %collective-permute-start.3 = (bf16[15,256]{1,0:T(8,128)(2,1)}, bf16[15,256]{1,0:T(8,128)(2,1)S(1)}, u32[]{:S(2)}, u32[]{:S(2)}) collective-permute-start(bf16[15,256]{1,0:T(8,128)(2,1)} %get-tuple-element.134), channel_id=1, source_target_pairs={{0,4},{4,8},{8,12},{12,16},{16,20},{20,24},{24,28},{1,5},{5,9},{9,... | collective-permute-start | bytes 23048 | tf_op jit(solution)/shard_map/ppermute | solution.py:22
  53.1 42.3 %collective-permute-start.4 = (bf16[15,256]{1,0:T(8,128)(2,1)}, bf16[15,256]{1,0:T(8,128)(2,1)}, u32[]{:S(2)}, u32[]{:S(2)}) collective-permute-start(bf16[15,256]{1,0:T(8,128)(2,1)} %get-tuple-element.135), channel_id=1, source_target_pairs={{4,0},{8,4},{12,8},{16,12},{20,16},{24,20},{28,24},{5,1},{9,5},{13... | collective-permute-start | bytes 23048 | tf_op jit(solution)/shard_map/ppermute | solution.py:23
  55.6 37.9 %copy-start.7 = (bf16[512,128]{1,0:T(8,128)(2,1)S(1)}, bf16[512,128]{1,0:T(8,128)(2,1)}, u32[]{:S(2)}) copy-start(bf16[512,128]{1,0:T(8,128)(2,1)} %param.32) | copy-start | bytes 393220
  55.6 37.9 %copy-start.10 = (f32[512]{0:T(512)S(1)}, f32[512]{0:T(512)}, u32[]{:S(2)}) copy-start(f32[512]{0:T(512)} %param.29) | copy-start | bytes 6148
  55.6 38.3 %copy-start.6 = (bf16[512,256]{1,0:T(8,128)(2,1)S(1)}, bf16[512,256]{1,0:T(8,128)(2,1)}, u32[]{:S(2)}) copy-start(bf16[512,256]{1,0:T(8,128)(2,1)} %param.31) | copy-start | bytes 786436
  111.0 18.7 %copy-start.1 = (bf16[512,256]{1,0:T(8,128)(2,1)S(1)}, bf16[512,256]{1,0:T(8,128)(2,1)}, u32[]{:S(2)}) copy-start(bf16[512,256]{1,0:T(8,128)(2,1)} %param.33) | copy-start | bytes 786436
  111.0 18.7 %copy-start.2 = (bf16[512,256]{1,0:T(8,128)(2,1)S(1)}, bf16[512,256]{1,0:T(8,128)(2,1)}, u32[]{:S(2)}) copy-start(bf16[512,256]{1,0:T(8,128)(2,1)} %param.34) | copy-start | bytes 786436
  174.2 36.1 %copy-start.9 = (f32[2048]{0:T(1024)S(1)}, f32[2048]{0:T(1024)}, u32[]{:S(2)}) copy-start(f32[2048]{0:T(1024)} %param.37) | copy-start | bytes 24580
Sparse Core Ops, SparseCore 0:
  42.6 80.6 all-gather.1
  178.9 30.0 reduce-scatter.1
